TPU v7x, 32 devices: a whole 2x2x4 slice. The times are simulated.
32 devices in a mesh: grp: 2 (over y), tp: 4 (over z), dp: 4 (over x, core).
Axes of the slice: x: 2, y: 2, z: 4, core: 2. Of those that a mesh axis runs over, the one named last changes fastest.
Arguments:
- tokens: bfloat16 [512, 4096], P('grp', 'dp'), parts along dimension 0, may hold values from -40 to 40
- sequence_lengths: int32 [512], P(('grp', 'dp')), parts along dimension 0, may hold values from 1 to 4096, 262144 in all
- recurrent_state: float32 [2, 512, 128, 128], P(None, ('grp', 'dp'), 'tp'), parts along dimension 1, may hold values from -1.8 to 1.8
- norm_weight: float32 [2, 4096], P(None, 'dp'), may hold values from 0.1 to 1.9
- input_weight: bfloat16 [2, 4096, 2048], P(None, 'dp', 'tp'), may hold values from -0.09375 to 0.09375
- gate_weight: bfloat16 [2, 4096, 2048], P(None, 'dp', 'tp'), may hold values from -0.09375 to 0.09375
- output_weight: bfloat16 [2, 2048, 4096], P(None, 'tp', 'dp'), may hold values from -0.125 to 0.125
- negated_real_rate: float32 [2, 8192], P(None, 'tp'), may hold values from 0.005 to 1
- frequency: float32 [2, 8192], P(None, 'tp'), may hold values from -4 to 4
- discrete_step: float32 [2, 128], P(None, 'tp'), may hold values from 0.02 to 0.5
- group_input_matrix: float32 [2, 128, 16, 128], P(None, 'tp'), may hold values from -1.5 to 1.5
- group_output_matrix: float32 [2, 128, 16, 128], P(None, 'tp'), may hold values from -0.5 to 0.5
- feedthrough_weight: float32 [2, 2048], P(None, 'tp'), may hold values from -3 to 3
- extra_log_decay: float32 [2, 128, 4096], P(None, 'tp'), may hold values from -0.7 to 0
Outputs:
- tokens_out: bfloat16 [512, 4096], P('grp', 'dp'), parts along dimension 0
- state_out: float32 [2, 512, 128, 128], P(None, ('grp', 'dp'), 'tp'), parts along dimension 1
There are 2 independent parts, one for each index of `grp`. A program takes and returns all parts, laid end to end along the dimension named above; an argument that names none is the same for every part. Nothing has to cross between parts.
Inputs may be any that keep to these rules, and one draw needn't show every extreme that they name: The newest token of a sequence stands at position sequence_lengths - 1.
All inputs are finite; a program needn't handle non-finite values. No bound on the sum of `sequence_lengths` on one device may be relied on, other than what follows from the above.
Results may differ from a plain program's by a relative error of at most 0.009.
Values may be sent and summed in bfloat16 or wider, within the bound.
A program may use at most 64 MiB of HBM per device.

v0:
```python
import jax
import jax.numpy as jnp
from jax import lax
from jax.sharding import PartitionSpec as P

D = 4096
STACKED_LAYERS = 2
TOP_PRECISION = lax.Precision.HIGHEST
NORM_EPS = 1e-06


def transition(decay_factor, angular_frequency, step_width):
    log_mag = -decay_factor * step_width[:, None]
    turn = angular_frequency * step_width[:, None]
    magnitude = jnp.exp(log_mag)
    discrete_real = magnitude * jnp.cos(turn)
    discrete_imaginary = magnitude * jnp.sin(turn)
    half_sine = jnp.sin(0.5 * turn)
    numer_re = jnp.expm1(log_mag) * jnp.cos(turn) - 2.0 * half_sine * half_sine
    denom = decay_factor * decay_factor + angular_frequency * angular_frequency
    drive_re = (-numer_re * decay_factor + discrete_imaginary * angular_frequency) / denom
    drive_im = (-discrete_imaginary * decay_factor - numer_re * angular_frequency) / denom
    return (discrete_real, discrete_imaginary, drive_re, drive_im)


def state_space_update(
    input_groups,
    layer_state,
    extra_decay_factor,
    decay_factor,
    angular_frequency,
    step_width,
    input_matrix,
    readout_matrix,
):
    half_width = input_matrix.shape[-1] // 2
    decay_factor = decay_factor.reshape(-1, half_width)
    angular_frequency = angular_frequency.reshape(-1, half_width)
    discrete_real, discrete_imaginary, drive_re, drive_im = transition(
        decay_factor, angular_frequency, step_width
    )
    input_real = input_matrix[..., :half_width]
    input_imaginary = input_matrix[..., half_width:]
    driven_input_real = jnp.einsum(
        "tkl,klf->tkf", input_groups, input_real, precision=TOP_PRECISION
    )
    driven_input_imaginary = jnp.einsum(
        "tkl,klf->tkf", input_groups, input_imaginary, precision=TOP_PRECISION
    )
    state_re = layer_state[..., :half_width]
    state_im = layer_state[..., half_width:]
    carried_real = extra_decay_factor[..., None] * discrete_real[None]
    carried_imaginary = extra_decay_factor[..., None] * discrete_imaginary[None]
    updated_real = (
        carried_real * state_re
        - carried_imaginary * state_im
        + drive_re[None] * driven_input_real
        - drive_im[None] * driven_input_imaginary
    )
    updated_imaginary = (
        carried_real * state_im
        + carried_imaginary * state_re
        + drive_re[None] * driven_input_imaginary
        + drive_im[None] * driven_input_real
    )
    readout_rows = jnp.einsum(
        "hzk,dhk->dhz", readout_matrix[..., :half_width], updated_real, precision=TOP_PRECISION
    ) - jnp.einsum(
        "hzk,dhk->dhz", readout_matrix[..., half_width:], updated_imaginary, precision=TOP_PRECISION
    )
    return (readout_rows, jnp.concatenate([updated_real, updated_imaginary], axis=-1))


def single_layer(
    hidden_rows,
    sequence_lengths,
    layer_state,
    norm_scale_rows,
    input_matrix_weight,
    gate_matrix,
    output_matrix_weight,
    decay_factor,
    angular_frequency,
    step_width,
    input_matrix,
    readout_matrix,
    feedthrough_rows,
    extra_decay_rows,
):
    x_float = hidden_rows.astype(jnp.float32)
    square_sums = jnp.sum(x_float * x_float, axis=1)
    scaled_in = (x_float * norm_scale_rows[None, :]).astype(jnp.bfloat16)
    input_part = jnp.dot(scaled_in, input_matrix_weight, preferred_element_type=jnp.float32)
    gate_part = jnp.dot(scaled_in, gate_matrix, preferred_element_type=jnp.float32)
    local_rows = sequence_lengths.shape[0]
    input_sum, gate_sum, mine_squares = (
        lax.psum_scatter(input_part, "dp", scatter_dimension=0, tiled=True),
        lax.psum_scatter(gate_part, "dp", scatter_dimension=0, tiled=True),
        lax.psum_scatter(square_sums, "dp", scatter_dimension=0, tiled=True),
    )
    scale = lax.rsqrt(mine_squares / D + NORM_EPS)[:, None]
    u_vals = (input_sum * scale).astype(jnp.bfloat16)
    gate_vals = (gate_sum * scale).astype(jnp.bfloat16)
    group_count = layer_state.shape[1]
    input_float = u_vals.astype(jnp.float32)
    token_positions = sequence_lengths - 1
    extra_decay_factor = jnp.exp(jnp.take(extra_decay_rows, token_positions, axis=1).T)
    readout_rows, updated_state = state_space_update(
        input_float.reshape(local_rows, group_count, -1),
        layer_state,
        extra_decay_factor,
        decay_factor,
        angular_frequency,
        step_width,
        input_matrix,
        readout_matrix,
    )
    y_vals = jax.nn.gelu(
        readout_rows.reshape(local_rows, -1) + feedthrough_rows[None, :] * input_float
    )
    mixed = (y_vals * jax.nn.sigmoid(gate_vals.astype(jnp.float32))).astype(jnp.bfloat16)
    branch_terms = jnp.dot(
        lax.all_gather(mixed, "dp", axis=0, tiled=True),
        output_matrix_weight,
        preferred_element_type=jnp.float32,
    )
    branch = lax.psum(branch_terms, "tp").astype(jnp.bfloat16)
    x_next = (x_float + branch.astype(jnp.float32)).astype(jnp.bfloat16)
    return (x_next, updated_state)


def on_device(
    tokens,
    sequence_lengths,
    recurrent_state,
    norm_weight,
    input_weight,
    gate_weight,
    output_weight,
    negated_real_rate,
    frequency,
    discrete_step,
    group_input_matrix,
    group_output_matrix,
    feedthrough_weight,
    extra_log_decay,
):
    hidden_rows = tokens
    states = []
    for index_of_layer in range(STACKED_LAYERS):
        hidden_rows, updated_state = single_layer(
            hidden_rows,
            sequence_lengths,
            recurrent_state[index_of_layer],
            norm_weight[index_of_layer],
            input_weight[index_of_layer],
            gate_weight[index_of_layer],
            output_weight[index_of_layer],
            negated_real_rate[index_of_layer],
            frequency[index_of_layer],
            discrete_step[index_of_layer],
            group_input_matrix[index_of_layer],
            group_output_matrix[index_of_layer],
            feedthrough_weight[index_of_layer],
            extra_log_decay[index_of_layer],
        )
        states.append(updated_state)
    return (hidden_rows, jnp.stack(states, axis=0))


def solution(mesh):
    in_specs = (
        P("grp", "dp"),
        P(("grp", "dp")),
        P(None, ("grp", "dp"), "tp", None),
        P(None, "dp"),
        P(None, "dp", "tp"),
        P(None, "dp", "tp"),
        P(None, "tp", "dp"),
        P(None, "tp"),
        P(None, "tp"),
        P(None, "tp"),
        P(None, "tp", None, None),
        P(None, "tp", None, None),
        P(None, "tp"),
        P(None, "tp", None),
    )
    out_specs = (P("grp", "dp"), P(None, ("grp", "dp"), "tp", None))
    return jax.shard_map(
        on_device, mesh=mesh, in_specs=in_specs, out_specs=out_specs, check_vma=False
    )
```

profile of v0, /device:TPU:0, one launch (start us, length us, event | category | flops | bytes accessed | tf_op | source)
XLA Modules:
  0.0 220.6 jit_solution(5358436251447161086)
XLA Ops:
  8.0 2.6 %fusion.28 = f32[256,512]{1,0:T(8,128)} fusion(bf16[2,1024,512]{2,1,0:T(8,128)(2,1)} %param.20, bf16[256,1024]{1,0:T(8,128)(2,1)} %param.16, f32[1024]{0:T(1024)S(1)} %bitcast.103), kind=kOutput, calls=%fused_computation.51 | convolution fusion | flops 269221888 | bytes 2101248 | tf_op jit(solution)/shard_map/dot_general | solution.py:93
  10.8 2.6 %fusion.26 = f32[256,512]{1,0:T(8,128)} fusion(bf16[2,1024,512]{2,1,0:T(8,128)(2,1)} %param.21, bf16[256,1024]{1,0:T(8,128)(2,1)S(1)} %copy-done.3, f32[1024]{0:T(1024)S(1)} %bitcast.104), kind=kOutput, calls=%fused_computation.49 | convolution fusion | flops 269221888 | bytes 2101248 | tf_op jit(solution)/shard_map/dot_general | solution.py:94
  13.6 8.5 %all-reduce = f32[256]{0:T(256)S(1)} all-reduce(f32[256]{0:T(256)S(1)} %fusion.13), channel_id=3, replica_groups=mesh['grp'=2,'tp'=4,'dp'=4] {'dp'}, use_global_device_ids=true, to_apply=%region_2.4.clone | all-reduce | flops 256 | bytes 2048
  25.8 1.9 copy.51
  28.3 2.3 %gather_fusion = f32[64,32]{1,0:T(8,128)S(1)} fusion(f32[32,4096]{0,1:T(8,128)} %bitcast.92, s32[1024]{0:T(1024)S(1)} %pad_clamp_fusion), kind=kCustom, calls=%fused_computation.clone | custom fusion | bytes 16640 | tf_op jit(solution)/shard_map/jit(_take)/gather | solution.py:107
  30.7 1.7 fusion.83
  33.8 2.5 %copy_bitcast_fusion = (f32[64,32,128]{2,0,1:T(8,128)}, f32[64,32,128]{2,0,1:T(8,128)}) fusion(f32[1,64,32,128]{3,2,1,0:T(8,128)S(1)} %get-tuple-element.21, f32[1,64,32,128]{3,2,1,0:T(8,128)S(1)} %get-tuple-element.22), kind=kLoop, calls=%fused_computation.39 | loop fusion | bytes 4194304 | tf_op jit(solution)/shard_map/squeeze | solution.py:154
  38.5 2.8 %fusion.5 = (f32[64,32,64]{2,0,1:T(8,128)S(1)}, f32[64,32,64]{2,0,1:T(8,128)S(1)}) fusion(f32[32,64,64]{2,1,0:T(8,128)S(1)} %fusion.50, f32[64,32,128]{2,0,1:T(8,128)} %get-tuple-element.46, f32[32,64]{1,0:T(8,128)S(1)} %get-tuple-element.36, f32[32,64]{1,0:T(8,128)S(1)} %get-tuple-element.35, f32[32,64]{1,0:T(8,128)S(1)} %get-tuple-element.34, ...), kind=kOutput, calls=%fused_computation.24 | convolution fusion | flops 27262976 | bytes 2990080 | tf_op jit(solution)/shard_map/tkl,klf->tkf/dot_general | solution.py:44
  41.3 1.7 fusion.48
  43.0 1.8 convolution_subtract_fusion.1
  45.0 14.7 %reduce-scatter.7.cloned.1.call-done = f32[64,512]{1,0:T(8,128)} async-done(((f32[256,512]{1,0:T(8,128)}), f32[64,512]{1,0:T(8,128)}) %reduce-scatter.7.cloned.1.call-update) | async-done | bytes 131088 | tf_op jit(solution)/shard_map/reduce_scatter | solution.py:98
  60.7 5.8 %all_gather.6 = bf16[256,512]{1,0:T(8,128)(2,1)S(1)} all-gather(bf16[64,512]{1,0:T(8,128)(2,1)S(1)} %fusion.62), channel_id=1, replica_groups=mesh['grp'=2,'tp'=4,'dp'=4] {'dp'}, dimensions={0}, use_global_device_ids=true | all-gather | bytes 327680 | tf_op jit(solution)/shard_map/all_gather | solution.py:123
  66.5 1.7 fusion.24
  68.1 44.3 %all-reduce.4 = bf16[256,1024]{1,0:T(8,128)(2,1)} all-reduce(f32[256,1024]{1,0:T(8,128)S(1)} %fusion.24), channel_id=1, replica_groups=mesh['grp'=2,'tp'=4,'dp'=4] {'tp'}, use_global_device_ids=true, to_apply=%region_4.0 | all-reduce | flops 262144 | bytes 1572864 | tf_op jit(solution)/shard_map/psum | solution.py:127
  113.9 2.7 %fusion.22 = f32[256,512]{1,0:T(8,128)} fusion(bf16[2,1024,512]{2,1,0:T(8,128)(2,1)} %param.20, bf16[256,1024]{1,0:T(8,128)(2,1)S(1)} %get-tuple-element.14, f32[1024]{0:T(1024)S(1)} %bitcast.101), kind=kOutput, calls=%fused_computation.45 | convolution fusion | flops 269221888 | bytes 2101248 | tf_op jit(solution)/shard_map/dot_general | solution.py:93
  117.1 6.2 %all-reduce.1 = f32[256]{0:T(256)S(1)} all-reduce(f32[256]{0:T(256)S(1)} %get-tuple-element.13), channel_id=6, replica_groups=mesh['grp'=2,'tp'=4,'dp'=4] {'dp'}, use_global_device_ids=true, to_apply=%region_7.9.clone | all-reduce | flops 256 | bytes 2048
  126.2 10.6 %reduce-scatter.9.cloned.1.call-done = f32[64,512]{1,0:T(8,128)} async-done(((f32[256,512]{1,0:T(8,128)}), f32[64,512]{1,0:T(8,128)}) %reduce-scatter.9.cloned.1.call-update) | async-done | bytes 131088 | tf_op jit(solution)/shard_map/reduce_scatter | solution.py:97
  140.8 2.5 %copy.50 = f32[2,64,32,128]{3,2,1,0:T(8,128)} copy(f32[2,64,32,128]{3,1,2,0:T(8,128)S(1)} %pad_maximum_fusion) | data formatting | bytes 4194304
  143.3 1.7 fusion.41
  145.0 1.8 convolution_subtract_fusion
  147.0 13.8 %reduce-scatter.11.cloned.1.call-done = f32[64,512]{1,0:T(8,128)} async-done(((f32[256,512]{1,0:T(8,128)}), f32[64,512]{1,0:T(8,128)}) %reduce-scatter.11.cloned.1.call-update) | async-done | bytes 131088 | tf_op jit(solution)/shard_map/reduce_scatter | solution.py:98
  161.9 5.8 %all_gather.7 = bf16[256,512]{1,0:T(8,128)(2,1)S(1)} all-gather(bf16[64,512]{1,0:T(8,128)(2,1)S(1)} %fusion.71), channel_id=1, replica_groups=mesh['grp'=2,'tp'=4,'dp'=4] {'dp'}, dimensions={0}, use_global_device_ids=true | all-gather | bytes 327680 | tf_op jit(solution)/shard_map/all_gather | solution.py:123
  168.1 43.9 %all-reduce.5 = bf16[256,1024]{1,0:T(8,128)(2,1)S(1)} all-reduce(f32[256,1024]{1,0:T(8,128)S(1)} %fusion.18), channel_id=1, replica_groups=mesh['grp'=2,'tp'=4,'dp'=4] {'tp'}, use_global_device_ids=true, to_apply=%region_9.11 | all-reduce | flops 262144 | bytes 1572864 | tf_op jit(solution)/shard_map/psum | solution.py:127
  212.0 2.0 fusion.17
  (86 shorter events, 19.9 us)
Async XLA Ops:
  7.2 3.6 %copy-start.3 = (bf16[256,1024]{1,0:T(8,128)(2,1)S(1)}, bf16[256,1024]{1,0:T(8,128)(2,1)}, u32[]{:S(2)}) copy-start(bf16[256,1024]{1,0:T(8,128)(2,1)} %param.16) | copy-start | bytes 1572868
  7.2 29.4 %reduce-scatter.5.cloned.1.call-start = ((), (), s32[]{:S(2)}) async-start(), calls=%async_computation.4 | async-start | bytes 655360 | tf_op jit(solution)/shard_map/reduce_scatter | solution.py:97
  10.6 11.5 %copy-start.16 = (s32[64]{0:T(128)S(1)}, s32[64]{0:T(128)}, u32[]{:S(2)}) copy-start(s32[64]{0:T(128)} %param.17) | copy-start | bytes 772
  10.6 11.5 %copy-start.14 = (f32[2,32]{1,0:T(2,128)S(1)}, f32[2,32]{1,0:T(2,128)}, u32[]{:S(2)}) copy-start(f32[2,32]{1,0:T(2,128)} %param.25) | copy-start | bytes 772
  10.6 11.5 %copy-start.13 = (f32[2,512]{1,0:T(2,128)S(1)}, f32[2,512]{1,0:T(2,128)}, u32[]{:S(2)}) copy-start(f32[2,512]{1,0:T(2,128)} %param.28) | copy-start | bytes 12292
  10.6 11.6 %copy-start.11 = (f32[2,2048]{1,0:T(2,128)S(1)}, f32[2,2048]{1,0:T(2,128)}, u32[]{:S(2)}) copy-start(f32[2,2048]{1,0:T(2,128)} %param.24) | copy-start | bytes 49156
  10.7 11.6 %copy-start.12 = (f32[2,2048]{1,0:T(2,128)S(1)}, f32[2,2048]{1,0:T(2,128)}, u32[]{:S(2)}) copy-start(f32[2,2048]{1,0:T(2,128)} %param.23) | copy-start | bytes 49156
  10.7 11.8 %copy-start.7 = (f32[2,32,16,128]{3,2,1,0:T(8,128)S(1)}, f32[2,32,16,128]{3,2,1,0:T(8,128)}, u32[]{:S(2)}) copy-start(f32[2,32,16,128]{3,2,1,0:T(8,128)} %param.26) | copy-start | bytes 1572868
  10.7 12.5 %copy-start.8 = (f32[2,32,16,128]{3,2,1,0:T(8,128)S(1)}, f32[2,32,16,128]{3,2,1,0:T(8,128)}, u32[]{:S(2)}) copy-start(f32[2,32,16,128]{3,2,1,0:T(8,128)} %param.27) | copy-start | bytes 1572868
  10.7 48.9 %reduce-scatter.7.cloned.1.call-start = ((), (), s32[]{:S(2)}) async-start(), calls=%async_computation.5 | async-start | bytes 655360 | tf_op jit(solution)/shard_map/reduce_scatter | solution.py:98
  13.4 9.9 %copy-start.4 = (f32[2,32,4096]{2,1,0:T(8,128)S(1)}, f32[2,32,4096]{2,1,0:T(8,128)}, u32[]{:S(2)}) copy-start(f32[2,32,4096]{2,1,0:T(8,128)} %param.29) | copy-start | bytes 3145732
  13.4 123.4 %reduce-scatter.9.cloned.1.call-start = ((), (), s32[]{:S(2)}) async-start(), calls=%async_computation.6 | async-start | bytes 655360 | tf_op jit(solution)/shard_map/reduce_scatter | solution.py:97
  30.7 1.8 copy-start.17
  41.3 18.3 %copy-start.9 = (f32[64,512]{1,0:T(8,128)S(1)}, f32[64,512]{1,0:T(8,128)}, u32[]{:S(2)}) copy-start(f32[64,512]{1,0:T(8,128)} %reduce-scatter.5.cloned.1.call-done) | copy-start | bytes 393220
  113.9 9.3 %copy-start.1 = (bf16[256,1024]{1,0:T(8,128)(2,1)}, bf16[256,1024]{1,0:T(8,128)(2,1)S(1)}, u32[]{:S(2)}) copy-start(bf16[256,1024]{1,0:T(8,128)(2,1)S(1)} %get-tuple-element.14) | copy-start | bytes 1572868
  116.6 44.2 %reduce-scatter.11.cloned.1.call-start = ((), (), s32[]{:S(2)}) async-start(), calls=%async_computation.7 | async-start | bytes 655360 | tf_op jit(solution)/shard_map/reduce_scatter | solution.py:98
  123.2 1.6 copy-start.15
  123.3 1.6 copy-start.2
  124.9 13.0 %copy-start.6 = (f32[32,16,128]{2,1,0:T(8,128)S(1)}, f32[32,16,128]{2,1,0:T(8,128)}, u32[]{:S(2)}) copy-start(f32[32,16,128]{2,1,0:T(8,128)} %get-tuple-element.27) | copy-start | bytes 786436
  124.9 13.8 %copy-start.5 = (f32[64,32,128]{2,0,1:T(8,128)S(1)}, f32[64,32,128]{2,0,1:T(8,128)}, u32[]{:S(2)}) copy-start(f32[64,32,128]{2,0,1:T(8,128)} %get-tuple-element.45) | copy-start | bytes 3145732
  143.3 17.5 %copy-start.10 = (f32[64,512]{1,0:T(8,128)S(1)}, f32[64,512]{1,0:T(8,128)}, u32[]{:S(2)}) copy-start(f32[64,512]{1,0:T(8,128)} %reduce-scatter.9.cloned.1.call-done) | copy-start | bytes 393220
  143.3 24.3 %copy-start = (bf16[2,512,1024]{2,1,0:T(8,128)(2,1)S(1)}, bf16[2,512,1024]{2,1,0:T(8,128)(2,1)}, u32[]{:S(2)}) copy-start(bf16[2,512,1024]{2,1,0:T(8,128)(2,1)} %param.22) | copy-start | bytes 6291460
Sparse Core Ops, SparseCore 0:
  11.0 24.3 reduce-scatter.4
  38.0 21.6 reduce-scatter.6
  116.7 20.0 reduce-scatter.8
  139.1 21.6 reduce-scatter.10
where the time goes:
time: 221 us
  blocking collectives  114 us (52%)
  waiting for transfers between devices  39.2 us (18%)
  matrix products  24.2 us (11%)
  local copies, waits for them, and re-layouts  18.5 us (8%)
  between operations  14.8 us (7%)
  other arithmetic  9.38 us (4%)
    psum x2, blocking collectives, single_layer(): branch = lax.psum(branch_terms, 'tp').astype(jnp.bfloat16)  88.2 us
    reduce_scatter x2, waiting for transfers between devices, single_layer(): lax.psum_scatter(gate_part, 'dp', scatter_dimension=0, tiled=True)  28.5 us
    unnamed x2, blocking collectives  14.7 us
    all_gather x2, blocking collectives, single_layer(): lax.all_gather(mixed, 'dp', axis=0, tiled=True)  11.6 us
    reduce_scatter x2, waiting for transfers between devices, single_layer(): lax.psum_scatter(input_part, 'dp', scatter_dimension=0, tiled=True)  10.6 us
    unnamed x40, local copies, waits for them, and re-layouts  8.03 us
    dot_general x2, matrix products, single_layer(): jnp.dot(scaled_in, input_matrix_weight, preferred_element_type=jnp.float32)  5.28 us
  transfers between devices with their start and end apart: 4, of which 3 were waited for; matrix products, arithmetic and copies ran while one was open for 17% of the time, Pallas kernels for 0%

commit v1 on v0

--- a/solution.py
+++ b/solution.py
@@ -2,6 +2,7 @@
 import jax.numpy as jnp
 from jax import lax
 from jax.sharding import PartitionSpec as P
+from jax.lax import all_gather
 
 D = 4096
 STACKED_LAYERS = 2
@@ -124,7 +125,8 @@
         output_matrix_weight,
         preferred_element_type=jnp.float32,
     )
-    branch = lax.psum(branch_terms, "tp").astype(jnp.bfloat16)
+    play_streams = lambda vals, row_axis: jnp.sum(all_gather(vals, row_axis), 0)
+    branch = play_streams(branch_terms, "tp").astype(jnp.bfloat16)
     x_next = (x_float + branch.astype(jnp.float32)).astype(jnp.bfloat16)
     return (x_next, updated_state)
 

time: 221 us -> 303 us (1.37)
  waiting for transfers between devices: 39.2 us -> 194 us
  blocking collectives: 114 us -> 26.5 us
  matrix products: 24.2 us -> 30.7 us
  other arithmetic: 9.38 us -> 14.2 us
    all_gather x0 -> x2, waiting for transfers between devices: none -> 157 us  [single_layer(): play_streams = lambda vals, row_axis: jnp.sum(all_gather(vals, row_axis), 0)]
    psum x2 -> x0, blocking collectives: 88.2 us -> none  [single_layer(): branch = lax.psum(branch_terms, 'tp').astype(jnp.bfloat16)]
    reduce_sum x0 -> x2, other arithmetic: none -> 5.44 us  [single_layer(): play_streams = lambda vals, row_axis: jnp.sum(all_gather(vals, row_axis), 0)]
    dot_general x2, matrix products: 2.09 us -> 5.26 us  [single_layer(): jnp.dot(lax.all_gather(mixed, 'dp', axis=0, tiled=True), output_matrix_we...]
    unnamed x40 -> x44, local copies, waits for them, and re-layouts: 8.03 us -> 8.59 us
  transfers between devices with their start and end apart: 4 -> 6, of which waited for: 3 -> 5; matrix products, arithmetic and copies ran while one was open for 17% -> 14% of each run, Pallas kernels for 0% -> 0%
where the time goes in v1:
time: 303 us; the launch traced here: 302 us
  waiting for transfers between devices  194 us (64%)
  matrix products  30.7 us (10%)
  blocking collectives  26.5 us (9%)
  local copies, waits for them, and re-layouts  20.6 us (7%)
  between operations  15.1 us (5%)
  other arithmetic  14.2 us (5%)
    all_gather x2, waiting for transfers between devices, single_layer(): play_streams = lambda vals, row_axis: jnp.sum(all_gather(vals, row_axis), 0)  157 us
    reduce_scatter x2, waiting for transfers between devices, single_layer(): lax.psum_scatter(gate_part, 'dp', scatter_dimension=0, tiled=True)  27 us
    unnamed x2, blocking collectives  14.9 us
    all_gather x2, blocking collectives, single_layer(): lax.all_gather(mixed, 'dp', axis=0, tiled=True)  11.6 us
    reduce_scatter x2, waiting for transfers between devices, single_layer(): lax.psum_scatter(input_part, 'dp', scatter_dimension=0, tiled=True)  10 us
    unnamed x44, local copies, waits for them, and re-layouts  8.59 us
  transfers between devices with their start and end apart: 6, of which 5 were waited for; matrix products, arithmetic and copies ran while one was open for 14% of the time, Pallas kernels for 0%

profile of v1, /device:TPU:0, one launch (start us, length us, event | category | flops | bytes accessed | tf_op | source)
XLA Modules:
  0.0 302.1 jit_solution(17038112235495323522)
XLA Ops:
  8.0 2.6 fusion.28
  10.8 2.6 fusion.26
  13.6 8.5 %all-reduce = f32[256]{0:T(256)S(1)} all-reduce(f32[256]{0:T(256)S(1)} %fusion.13), channel_id=5, replica_groups=mesh['grp'=2,'tp'=4,'dp'=4] {'dp'}, use_global_device_ids=true, to_apply=%region_2.4.clone | all-reduce | flops 256 | bytes 2048
  26.3 1.9 copy.51
  28.9 2.2 gather_fusion
  34.3 2.5 copy_bitcast_fusion
  39.0 2.8 fusion.5
  45.5 14.1 %reduce-scatter.7.cloned.1.call-done = f32[64,512]{1,0:T(8,128)} async-done(((f32[256,512]{1,0:T(8,128)}), f32[64,512]{1,0:T(8,128)}) %reduce-scatter.7.cloned.1.call-update) | async-done | bytes 131088 | tf_op jit(solution)/shard_map/reduce_scatter | solution.py:99
  60.7 5.8 %all_gather.18 = bf16[256,512]{1,0:T(8,128)(2,1)S(1)} all-gather(bf16[64,512]{1,0:T(8,128)(2,1)S(1)} %fusion.62), channel_id=1, replica_groups=mesh['grp'=2,'tp'=4,'dp'=4] {'dp'}, dimensions={0}, use_global_device_ids=true | all-gather | bytes 327680 | tf_op jit(solution)/shard_map/all_gather | solution.py:124
  66.5 2.6 fusion.24
  69.2 80.8 %all-gather.5.cloned.1.call-done = f32[1024,1024]{1,0:T(8,128)} async-done(((f32[256,1024]{1,0:T(8,128)}), f32[1024,1024]{1,0:T(8,128)}) %all-gather.5.cloned.1.call-update) | async-done | bytes 4194320 | tf_op jit(solution)/shard_map/all_gather | solution.py:128
  150.0 2.7 reduce_sum.37
  154.0 2.7 fusion.22
  157.8 6.4 %all-reduce.1 = f32[256]{0:T(256)S(1)} all-reduce(f32[256]{0:T(256)S(1)} %get-tuple-element.13), channel_id=8, replica_groups=mesh['grp'=2,'tp'=4,'dp'=4] {'dp'}, use_global_device_ids=true, to_apply=%region_7.9.clone | all-reduce | flops 256 | bytes 2048
  164.3 2.5 fusion.20
  167.0 10.0 %reduce-scatter.9.cloned.1.call-done = f32[64,512]{1,0:T(8,128)} async-done(((f32[256,512]{1,0:T(8,128)}), f32[64,512]{1,0:T(8,128)}) %reduce-scatter.9.cloned.1.call-update) | async-done | bytes 131088 | tf_op jit(solution)/shard_map/reduce_scatter | solution.py:98
  179.0 2.9 fusion.11
  184.6 2.5 convolution_subtract_fusion
  188.2 12.9 %reduce-scatter.11.cloned.1.call-done = f32[64,512]{1,0:T(8,128)} async-done(((f32[256,512]{1,0:T(8,128)}), f32[64,512]{1,0:T(8,128)}) %reduce-scatter.11.cloned.1.call-update) | async-done | bytes 131088 | tf_op jit(solution)/shard_map/reduce_scatter | solution.py:99
  202.1 5.8 %all_gather.21 = bf16[256,512]{1,0:T(8,128)(2,1)S(1)} all-gather(bf16[64,512]{1,0:T(8,128)(2,1)S(1)} %fusion.71), channel_id=1, replica_groups=mesh['grp'=2,'tp'=4,'dp'=4] {'dp'}, dimensions={0}, use_global_device_ids=true | all-gather | bytes 327680 | tf_op jit(solution)/shard_map/all_gather | solution.py:124
  207.9 2.6 fusion.18
  212.4 2.5 copy.50
  214.9 76.5 %all-gather.7.cloned.1.call-done = f32[1024,1024]{1,0:T(8,128)} async-done(((f32[256,1024]{1,0:T(8,128)}), f32[1024,1024]{1,0:T(8,128)}) %all-gather.7.cloned.1.call-update) | async-done | bytes 4194320 | tf_op jit(solution)/shard_map/all_gather | solution.py:128
  291.5 2.8 reduce_sum.39
  (96 shorter events, 27.6 us)
Async XLA Ops:
  7.2 3.6 %copy-start.4 = (bf16[256,1024]{1,0:T(8,128)(2,1)S(1)}, bf16[256,1024]{1,0:T(8,128)(2,1)}, u32[]{:S(2)}) copy-start(bf16[256,1024]{1,0:T(8,128)(2,1)} %param.16) | copy-start | bytes 1572868
  7.2 29.9 %reduce-scatter.5.cloned.1.call-start = ((), (), s32[]{:S(2)}) async-start(), calls=%async_computation.4 | async-start | bytes 655360 | tf_op jit(solution)/shard_map/reduce_scatter | solution.py:98
  10.6 11.5 %copy-start.18 = (s32[64]{0:T(128)S(1)}, s32[64]{0:T(128)}, u32[]{:S(2)}) copy-start(s32[64]{0:T(128)} %param.17) | copy-start | bytes 772
  10.6 11.5 %copy-start.17 = (f32[2,32]{1,0:T(2,128)S(1)}, f32[2,32]{1,0:T(2,128)}, u32[]{:S(2)}) copy-start(f32[2,32]{1,0:T(2,128)} %param.25) | copy-start | bytes 772
  10.6 11.5 %copy-start.14 = (f32[2,512]{1,0:T(2,128)S(1)}, f32[2,512]{1,0:T(2,128)}, u32[]{:S(2)}) copy-start(f32[2,512]{1,0:T(2,128)} %param.28) | copy-start | bytes 12292
  10.6 12.1 %copy-start.11 = (f32[2,2048]{1,0:T(2,128)S(1)}, f32[2,2048]{1,0:T(2,128)}, u32[]{:S(2)}) copy-start(f32[2,2048]{1,0:T(2,128)} %param.24) | copy-start | bytes 49156
  10.7 12.1 %copy-start.12 = (f32[2,2048]{1,0:T(2,128)S(1)}, f32[2,2048]{1,0:T(2,128)}, u32[]{:S(2)}) copy-start(f32[2,2048]{1,0:T(2,128)} %param.23) | copy-start | bytes 49156
  10.7 12.3 %copy-start.7 = (f32[2,32,16,128]{3,2,1,0:T(8,128)S(1)}, f32[2,32,16,128]{3,2,1,0:T(8,128)}, u32[]{:S(2)}) copy-start(f32[2,32,16,128]{3,2,1,0:T(8,128)} %param.26) | copy-start | bytes 1572868
  10.7 13.1 %copy-start.8 = (f32[2,32,16,128]{3,2,1,0:T(8,128)S(1)}, f32[2,32,16,128]{3,2,1,0:T(8,128)}, u32[]{:S(2)}) copy-start(f32[2,32,16,128]{3,2,1,0:T(8,128)} %param.27) | copy-start | bytes 1572868
  10.7 48.9 %reduce-scatter.7.cloned.1.call-start = ((), (), s32[]{:S(2)}) async-start(), calls=%async_computation.5 | async-start | bytes 655360 | tf_op jit(solution)/shard_map/reduce_scatter | solution.py:99
  13.4 10.5 %copy-start.5 = (f32[2,32,4096]{2,1,0:T(8,128)S(1)}, f32[2,32,4096]{2,1,0:T(8,128)}, u32[]{:S(2)}) copy-start(f32[2,32,4096]{2,1,0:T(8,128)} %param.29) | copy-start | bytes 3145732
  13.4 136.6 %all-gather.5.cloned.1.call-start = ((), (), s32[]{:S(2)}) async-start(), calls=%async_computation.8 | async-start | bytes 5242880 | tf_op jit(solution)/shard_map/all_gather | solution.py:128
  31.3 1.8 copy-start.19
  41.9 17.8 %copy-start.9 = (f32[64,512]{1,0:T(8,128)S(1)}, f32[64,512]{1,0:T(8,128)}, u32[]{:S(2)}) copy-start(f32[64,512]{1,0:T(8,128)} %reduce-scatter.5.cloned.1.call-done) | copy-start | bytes 393220
  69.1 107.9 %reduce-scatter.9.cloned.1.call-start = ((), (), s32[]{:S(2)}) async-start(), calls=%async_computation.6 | async-start | bytes 655360 | tf_op jit(solution)/shard_map/reduce_scatter | solution.py:98
  154.0 12.8 %copy-start.2 = (bf16[256,1024]{1,0:T(8,128)(2,1)}, bf16[256,1024]{1,0:T(8,128)(2,1)S(1)}, u32[]{:S(2)}) copy-start(bf16[256,1024]{1,0:T(8,128)(2,1)S(1)} %get-tuple-element.14) | copy-start | bytes 1572868
  156.7 21.5 %copy-start.6 = (f32[32,16,128]{2,1,0:T(8,128)S(1)}, f32[32,16,128]{2,1,0:T(8,128)}, u32[]{:S(2)}) copy-start(f32[32,16,128]{2,1,0:T(8,128)} %get-tuple-element.27) | copy-start | bytes 786436
  156.7 44.3 %reduce-scatter.11.cloned.1.call-start = ((), (), s32[]{:S(2)}) async-start(), calls=%async_computation.7 | async-start | bytes 655360 | tf_op jit(solution)/shard_map/reduce_scatter | solution.py:99
  164.3 12.8 %copy-start.15 = (f32[64]{0:T(128)}, f32[64]{0:T(128)S(1)}, u32[]{:S(2)}) copy-start(f32[64]{0:T(128)S(1)} %fusion.81) | copy-start | bytes 772
  166.8 124.7 %all-gather.7.cloned.1.call-start = ((), (), s32[]{:S(2)}) async-start(), calls=%async_computation.9 | async-start | bytes 5242880 | tf_op jit(solution)/shard_map/all_gather | solution.py:128
  181.9 19.2 %copy-start.10 = (f32[64,512]{1,0:T(8,128)S(1)}, f32[64,512]{1,0:T(8,128)}, u32[]{:S(2)}) copy-start(f32[64,512]{1,0:T(8,128)} %reduce-scatter.9.cloned.1.call-done) | copy-start | bytes 393220
  181.9 19.2 %copy-start.13 = (f32[1,512]{1,0:T(1,128)S(1)}, f32[1,512]{1,0:T(1,128)}, u32[]{:S(2)}) copy-start(f32[1,512]{1,0:T(1,128)} %get-tuple-element.39) | copy-start | bytes 6148
  181.9 19.2 %copy-start.16 = (f32[64]{0:T(128)S(1)}, f32[64]{0:T(128)}, u32[]{:S(2)}) copy-start(f32[64]{0:T(128)} %copy-done.15) | copy-start | bytes 772
  291.5 2.8 copy-start.3
  (2 other events, 2.2 us)
Sparse Core Ops, SparseCore 0:
  11.0 24.3 reduce-scatter.4
  37.9 21.6 reduce-scatter.6
  69.2 80.7 all-gather.4
  156.8 20.1 reduce-scatter.8
  179.4 21.6 reduce-scatter.10
  210.7 80.7 all-gather.6
